TPU v7x, 32 devices: a whole 2x2x4 slice. The times are simulated.
32 devices in a mesh: sp: 8 (over z, y), tp: 4 (over x, core).
Axes of the slice: x: 2, y: 2, z: 4, core: 2. Of those that a mesh axis runs over, the one named last changes fastest.
Arguments:
- query: bfloat16 [2048, 1536], P('sp', 'tp'), may hold values from -6 to 6
- forget_preact: bfloat16 [2048, 1536], P('sp', 'tp'), may hold values from -6 to 6
- value_input: bfloat16 [2048, 1536], P('sp', 'tp'), may hold values from -6 to 6
- output_gate: bfloat16 [2048, 1536], P('sp', 'tp'), may hold values from -6 to 6
- forget_minimum: float32 [1536], P('tp'), may hold values from 0.88 to 1
- extra_log_decay: float32 [12, 2048], P('tp', 'sp'), may hold values from -0.7 to 0
- head_norm_gain: float32 [1536], P('tp'), may hold values from 0.1 to 1.9
- output_weight: bfloat16 [1536, 3072], P(None, 'tp'), may hold values from -0.15625 to 0.15625
- stream: bfloat16 [2048, 3072], P(('sp', 'tp')), may hold values from -6 to 6
- feedforward_gain: float32 [3072], replicated, may hold values from 0.1 to 1.9
- routes: int32 [2048, 2], P('sp'), may hold values from 0 to 7, all different within a row; in each aligned block of 64 rows (0 to 63, 64 to 127, ...) at most 32 rows name the same one
- router_weight: float32 [2048, 2], P(('sp', 'tp')), may hold values from 0.05 to 1
- expert_gate_weight: bfloat16 [8, 3072, 1024], P('sp', None, 'tp'), may hold values from -0.109375 to 0.109375
- expert_up_weight: bfloat16 [8, 3072, 1024], P('sp', None, 'tp'), may hold values from -0.109375 to 0.109375
- expert_down_weight: bfloat16 [8, 1024, 3072], P('sp', 'tp'), may hold values from -0.1875 to 0.1875
Outputs:
- result: bfloat16 [2048, 3072], P(('sp', 'tp'))
Inputs may be any that keep to these rules, and one draw needn't show every extreme that they name: `routes`: each row names 2 different experts; in each aligned block of 64 rows no expert is named by more than 32 rows, a bound that some block reaches.
All inputs are finite; a program needn't handle non-finite values.
Results may differ from a plain program's by a relative error of at most 0.01.
Values may be sent and summed in bfloat16 or wider, within the bound.
A program may use at most 64 MiB of HBM per device.

v0:
```python
import functools

import jax
import jax.numpy as jnp
from jax import lax
from jax.experimental import pallas as pl
from jax.experimental.pallas import tpu as pltpu
from jax.sharding import PartitionSpec as P

STATE_ROW_COUNT = 128
VALUE_CHANNELS = 128
SPAN = 64
TOPK = 2


epsilon = 1e-06
MESH = pl.DeviceIdType.MESH


def silu(x):
    return x / (1.0 + jnp.exp(-x))


def nt_dot(a, b):
    return lax.dot_general(a, b, (((1,), (1,)), ((), ())), preferred_element_type=jnp.float32)


def tn_dot(a, b):
    return lax.dot_general(a, b, (((0,), (0,)), ((), ())), preferred_element_type=jnp.float32)


def mixer_kernel(
    sp_size,
    tp_size,
    q_ref,
    f_ref,
    v_ref,
    g_ref,
    fmin_ref,
    extra_ref,
    gain_ref,
    wo_ref,
    stream_ref,
    ffgain_ref,
    residual_ref,
    normed_ref,
    local_ref,
    qtot_ref,
    incl_ref,
    incl_dec_ref,
    excl_ref,
    excl_dec_ref,
    st_send,
    st_recv,
    hid_ref,
    acc_ref,
    proj_ref,
    cols_ref,
    st_send_sem,
    st_recv_sem,
    hid_send_sem,
    hid_recv_sem,
    col_send_sem,
    col_recv_sem,
):
    sp_me, tp_me = lax.axis_index("sp"), lax.axis_index("tp")
    rows, width = q_ref.shape
    lanes = STATE_ROW_COUNT
    heads = width // lanes
    spans = rows // SPAN
    state_rows = heads * lanes
    distances = []
    while (1 << len(distances)) < sp_size:
        distances.append(1 << len(distances))

    barrier = pltpu.get_barrier_semaphore()
    expected = tp_size - 1
    for d in distances:
        has_next = sp_me + d < sp_size
        has_prev = sp_me >= d
        expected = expected + has_next.astype(jnp.int32) + has_prev.astype(jnp.int32)

        @pl.when(has_next)
        def _():
            pl.semaphore_signal(
                barrier, inc=1, device_id=(sp_me + d, tp_me), device_id_type=MESH
            )

        @pl.when(has_prev)
        def _():
            pl.semaphore_signal(
                barrier, inc=1, device_id=(sp_me - d, tp_me), device_id_type=MESH
            )

    for o in range(1, tp_size):
        pl.semaphore_signal(
            barrier,
            inc=1,
            device_id=(sp_me, lax.rem(tp_me + o, tp_size)),
            device_id_type=MESH,
        )

    causal = lax.broadcasted_iota(jnp.int32, (SPAN, SPAN), 0) >= lax.broadcasted_iota(
        jnp.int32, (SPAN, SPAN), 1
    )
    ones_low = jnp.where(causal, 1.0, 0.0).astype(jnp.float32)
    incl_dec_ref[...] = jnp.zeros_like(incl_dec_ref)
    for h in range(heads):
        cols = slice(h * lanes, (h + 1) * lanes)
        state = jnp.zeros((lanes, lanes), jnp.float32)
        base = jnp.zeros((1, lanes), jnp.float32)
        floor_gap = 1.0 - fmin_ref[:, cols]
        for c in range(spans):
            at = slice(c * SPAN, (c + 1) * SPAN)
            query = silu(q_ref[at, cols].astype(jnp.float32))
            weight = floor_gap / (1.0 + jnp.exp(f_ref[at, cols].astype(jnp.float32)))
            log_decay = jnp.log(1.0 - weight) + extra_ref[at, h : h + 1]
            running = jnp.dot(
                ones_low,
                log_decay,
                precision=lax.Precision.HIGHEST,
                preferred_element_type=jnp.float32,
            )
            final = running[SPAN - 1 : SPAN, :]
            value = v_ref[at, cols]
            q_dec = query * jnp.exp(running)
            q_low = q_dec.astype(jnp.bfloat16)
            k_low = (weight * jnp.exp(-running)).astype(jnp.bfloat16)
            k_end = (weight * jnp.exp(final - running)).astype(jnp.bfloat16)
            scores = jnp.where(causal, nt_dot(q_low, k_low), 0.0).astype(jnp.bfloat16)
            out = jnp.dot(scores, value, preferred_element_type=jnp.float32)
            if c:
                out = out + nt_dot(q_low, state.astype(jnp.bfloat16))
            local_ref[at, cols] = out
            qtot_ref[at, cols] = (q_dec * jnp.exp(base)).astype(jnp.bfloat16)
            state = jnp.exp(final) * state + tn_dot(value, k_end)
            base = base + final
        incl_ref[h * lanes : (h + 1) * lanes, :] = state
        incl_dec_ref[h : h + 1, :] = base

    excl_ref[...] = jnp.zeros_like(excl_ref)
    excl_dec_ref[...] = jnp.zeros_like(excl_dec_ref)
    pl.semaphore_wait(barrier, expected)

    def state_copy(r):
        return pltpu.make_async_remote_copy(
            src_ref=st_send.at[r],
            dst_ref=st_recv.at[r],
            send_sem=st_send_sem.at[r],
            recv_sem=st_recv_sem.at[r],
            device_id=(lax.rem(sp_me + distances[r], sp_size), tp_me),
            device_id_type=MESH,
        )

    for r, d in enumerate(distances):
        st_send[r, :state_rows, :] = incl_ref[...].astype(jnp.bfloat16)
        st_send[r, state_rows:, :] = incl_dec_ref[...].astype(jnp.bfloat16)

        @pl.when(sp_me + d < sp_size)
        def _():
            state_copy(r).start()

        @pl.when(sp_me >= d)
        def _():
            state_copy(r).wait_recv()
            earlier_dec = st_recv[r, state_rows:, :].astype(jnp.float32)
            for h in range(heads):
                at = slice(h * lanes, (h + 1) * lanes)
                earlier = st_recv[r, at, :].astype(jnp.float32)
                excl_ref[at, :] = excl_ref[at, :] + earlier * jnp.exp(excl_dec_ref[h : h + 1, :])
                if d != distances[-1]:
                    incl_ref[at, :] = incl_ref[at, :] + earlier * jnp.exp(
                        incl_dec_ref[h : h + 1, :]
                    )
            excl_dec_ref[...] = excl_dec_ref[...] + earlier_dec
            incl_dec_ref[...] = incl_dec_ref[...] + earlier_dec

    for h in range(heads):
        cols = slice(h * lanes, (h + 1) * lanes)
        carried = excl_ref[cols, :].astype(jnp.bfloat16)
        mixed = local_ref[:, cols] + nt_dot(qtot_ref[:, cols], carried)
        mean = jnp.mean(mixed * mixed, axis=-1, keepdims=True)
        normalized = mixed * lax.rsqrt(mean + epsilon)
        gated = normalized * gain_ref[:, cols] * silu(g_ref[:, cols].astype(jnp.float32))
        hid_ref[tp_me, :, cols] = gated.astype(jnp.bfloat16)

    def hidden_copy(o, source):
        return pltpu.make_async_remote_copy(
            src_ref=hid_ref.at[source],
            dst_ref=hid_ref.at[source],
            send_sem=hid_send_sem.at[o],
            recv_sem=hid_recv_sem.at[o],
            device_id=(sp_me, lax.rem(tp_me + o, tp_size)),
            device_id_type=MESH,
        )

    for o in range(1, tp_size):
        hidden_copy(o, tp_me).start()

    def part(source):
        at = pl.ds(pl.multiple_of(source * width, width), width)
        return jnp.dot(hid_ref[source], wo_ref[at, :], preferred_element_type=jnp.float32)

    acc_ref[...] = part(tp_me)
    for o in range(1, tp_size):
        source = lax.rem(tp_me + tp_size - o, tp_size)
        hidden_copy(o, source).wait_recv()
        acc_ref[...] += part(source)
    own_rows = residual_ref.shape[0]
    for p in range(tp_size):
        proj_ref[p] = acc_ref[p * own_rows : (p + 1) * own_rows, :].astype(jnp.bfloat16)

    def column_copy(o, source):
        return pltpu.make_async_remote_copy(
            src_ref=proj_ref.at[lax.rem(tp_me + o, tp_size)],
            dst_ref=cols_ref.at[source],
            send_sem=col_send_sem.at[o],
            recv_sem=col_recv_sem.at[o],
            device_id=(sp_me, lax.rem(tp_me + o, tp_size)),
            device_id_type=MESH,
        )

    for o in range(1, tp_size):
        column_copy(o, tp_me).start()
    cols_ref[tp_me] = proj_ref[tp_me]
    for o in range(1, tp_size):
        column_copy(o, lax.rem(tp_me + tp_size - o, tp_size)).wait_recv()
    part_width = cols_ref.shape[2]
    squares = jnp.zeros((own_rows, 1), jnp.float32)
    for p in range(tp_size):
        cols = slice(p * part_width, (p + 1) * part_width)
        residual = stream_ref[:, cols].astype(jnp.float32) + cols_ref[p].astype(jnp.float32)
        residual_ref[:, cols] = residual
        squares = squares + jnp.sum(residual * residual, axis=-1, keepdims=True)
    scale = lax.rsqrt(squares / (part_width * tp_size) + epsilon)
    normed_ref[...] = (residual_ref[...] * scale * ffgain_ref[...]).astype(jnp.bfloat16)

    for r, d in enumerate(distances):

        @pl.when(sp_me + d < sp_size)
        def _():
            state_copy(r).wait_send()

    for o in range(1, tp_size):
        hidden_copy(o, tp_me).wait_send()
        column_copy(o, tp_me).wait_send()


def mixer(
    query,
    forget_preact,
    value_input,
    output_gate,
    forget_minimum,
    extra_log_decay,
    head_norm_gain,
    output_weight,
    stream,
    feedforward_gain,
):
    sp_size, tp_size = lax.axis_size("sp"), lax.axis_size("tp")
    rows, width = query.shape
    heads = width // STATE_ROW_COUNT
    own_rows, model_width = stream.shape
    rounds = max(1, (sp_size - 1).bit_length())
    state_rows = heads * STATE_ROW_COUNT
    dec_rows = -(-heads // 16) * 16
    lanes = VALUE_CHANNELS
    columns = output_weight.shape[1]
    vmem = pl.BlockSpec(memory_space=pltpu.VMEM)
    dma = pltpu.SemaphoreType.DMA
    return pl.pallas_call(
        functools.partial(mixer_kernel, sp_size, tp_size),
        out_shape=(
            jax.ShapeDtypeStruct((own_rows, model_width), jnp.float32),
            jax.ShapeDtypeStruct((own_rows, model_width), jnp.bfloat16),
        ),
        in_specs=[vmem] * 10,
        out_specs=(vmem, vmem),
        scratch_shapes=[
            pltpu.VMEM((rows, width), jnp.float32),
            pltpu.VMEM((rows, width), jnp.bfloat16),
            pltpu.VMEM((state_rows, lanes), jnp.float32),
            pltpu.VMEM((dec_rows, lanes), jnp.float32),
            pltpu.VMEM((state_rows, lanes), jnp.float32),
            pltpu.VMEM((dec_rows, lanes), jnp.float32),
            pltpu.VMEM((rounds, state_rows + dec_rows, lanes), jnp.bfloat16),
            pltpu.VMEM((rounds, state_rows + dec_rows, lanes), jnp.bfloat16),
            pltpu.VMEM((tp_size, rows, width), jnp.bfloat16),
            pltpu.VMEM((rows, columns), jnp.float32),
            pltpu.VMEM((tp_size, own_rows, columns), jnp.bfloat16),
            pltpu.VMEM((tp_size, own_rows, columns), jnp.bfloat16),
            dma((rounds,)),
            dma((rounds,)),
            dma((tp_size,)),
            dma((tp_size,)),
            dma((tp_size,)),
            dma((tp_size,)),
        ],
        compiler_params=pltpu.CompilerParams(collective_id=0, has_side_effects=True),
        cost_estimate=pl.CostEstimate(
            flops=2 * rows * width * tp_size * columns,
            bytes_accessed=2 * (output_weight.size + 8 * query.size),
            transcendentals=6 * query.size,
        ),
        name="mixer",
    )(
        query,
        forget_preact,
        value_input,
        output_gate,
        forget_minimum[None],
        jnp.transpose(extra_log_decay),
        head_norm_gain[None],
        output_weight,
        stream,
        feedforward_gain[None],
    )


def dispatch_table(slot_ids, window_rows, quarter_rows):
    groups = slot_ids.shape[0]
    slot_grid = lax.broadcasted_iota(jnp.int32, (groups, window_rows, slot_ids.shape[1]), 1)
    hits = (slot_grid == slot_ids[:, None, :]).astype(jnp.bfloat16)
    return jnp.sum(hits.reshape(groups, window_rows, quarter_rows, TOPK), axis=3)


def per_device(
    query,
    forget_preact,
    value_input,
    output_gate,
    forget_minimum,
    extra_log_decay,
    head_norm_gain,
    output_weight,
    stream,
    feedforward_gain,
    routes,
    router_weight,
    expert_gate_weight,
    expert_up_weight,
    expert_down_weight,
):
    window_rows = query.shape[0]
    tp_size = lax.axis_size("tp")
    sp_size = lax.axis_size("sp")
    gate_all = lax.all_gather(expert_gate_weight[0], "tp")
    up_all = lax.all_gather(expert_up_weight[0], "tp")
    down_all = lax.all_gather(expert_down_weight[0], "tp")
    residual, normed = mixer(
        query,
        forget_preact,
        value_input,
        output_gate,
        forget_minimum,
        extra_log_decay,
        head_norm_gain,
        output_weight,
        stream,
        feedforward_gain,
    )
    quarter_rows = stream.shape[0]
    capacity = window_rows // sp_size
    pick_ids = routes.reshape(tp_size, quarter_rows * TOPK)
    onehot = (pick_ids[:, :, None] == jnp.arange(sp_size, dtype=jnp.int32)[None, None, :]).astype(
        jnp.int32
    )
    rank_ids = jnp.sum((jnp.cumsum(onehot, axis=1) - 1) * onehot, axis=2)
    slot_ids = pick_ids * capacity + rank_ids
    own_index = lax.axis_index("tp")
    own_slots = lax.dynamic_slice_in_dim(slot_ids, own_index, 1, 0)
    send_table = dispatch_table(own_slots, window_rows, quarter_rows)[0]
    sendbuf = jnp.dot(send_table, normed, preferred_element_type=jnp.float32).astype(jnp.bfloat16)
    received = lax.all_to_all(
        sendbuf.reshape(sp_size, capacity, -1), "sp", split_axis=0, concat_axis=0, tiled=True
    )
    flat_rows = received.reshape(window_rows, -1)
    gate_act = jnp.einsum("nd,tdf->tnf", flat_rows, gate_all, preferred_element_type=jnp.float32)
    up_act = jnp.einsum("nd,tdf->tnf", flat_rows, up_all, preferred_element_type=jnp.float32)
    inner_act = (jax.nn.silu(gate_act) * up_act).astype(jnp.bfloat16)
    inner_all = jnp.transpose(inner_act, (1, 0, 2)).reshape(window_rows, -1)
    down_flat = down_all.reshape(-1, down_all.shape[-1])
    expert_out = jnp.dot(inner_all, down_flat, preferred_element_type=jnp.float32).astype(
        jnp.bfloat16
    )
    returned = lax.all_to_all(
        expert_out.reshape(sp_size, capacity, -1), "sp", split_axis=0, concat_axis=0, tiled=True
    )
    results = returned.reshape(window_rows, -1)
    route_weight = router_weight / jnp.sum(router_weight, axis=1, keepdims=True)
    row_slots = own_slots.reshape(quarter_rows, TOPK)
    slot_grid = lax.broadcasted_iota(jnp.int32, (quarter_rows, TOPK, window_rows), 2)
    table = jnp.sum(
        jnp.where(slot_grid == row_slots[:, :, None], route_weight[:, :, None], 0.0), axis=1
    )
    table_high = table.astype(jnp.bfloat16)
    table_low = (table - table_high.astype(jnp.float32)).astype(jnp.bfloat16)
    routed_sum = jnp.dot(table_high, results, preferred_element_type=jnp.float32) + jnp.dot(
        table_low, results, preferred_element_type=jnp.float32
    )
    return (residual + routed_sum).astype(jnp.bfloat16)


def solution(mesh):
    placed = (
        P("sp", "tp"),
        P("sp", "tp"),
        P("sp", "tp"),
        P("sp", "tp"),
        P("tp"),
        P("tp", "sp"),
        P("tp"),
        P(None, "tp"),
        P(("sp", "tp"), None),
        P(),
        P("sp", None),
        P(("sp", "tp"), None),
        P("sp", None, "tp"),
        P("sp", None, "tp"),
        P("sp", "tp", None),
    )
    return jax.shard_map(
        per_device, mesh=mesh, in_specs=placed, out_specs=P(("sp", "tp"), None), check_vma=False
    )
```

profile of v0, /device:TPU:0, one launch (start us, length us, event | category | flops | bytes accessed | tf_op | source)
XLA Modules:
  0.0 227.1 jit_solution(13793894290435431900)
XLA Ops:
  6.5 0.0 all-gather.4.cloned.1.call-start
  6.5 0.7 all-gather.4.cloned.1.call-update
  7.3 0.0 all-gather.6.cloned.1.call-start
  7.3 0.7 all-gather.6.cloned.1.call-update
  8.0 0.0 all-gather.8.cloned.1.call-start
  8.1 0.7 all-gather.8.cloned.1.call-update
  8.8 0.0 copy-done.3
  8.8 0.1 copy.25
  8.9 0.1 reshape.52
  9.1 0.1 fusion.5
  9.2 0.3 reduce_window_sum.11
  9.5 0.2 select_reduce_fusion
  9.8 0.1 eq.43
  9.9 0.1 copy.26
  10.0 0.8 copy.24
  10.8 0.6 broadcast_in_dim.25.fmin_ref
  11.4 0.0 copy-done.5
  11.4 0.6 broadcast_in_dim.26.gain_ref
  12.0 32.9 %mixer.1 = (f32[64,3072]{1,0:T(8,128)}, bf16[64,3072]{1,0:T(8,128)(2,1)}) custom-call(bf16[256,384]{1,0:T(8,128)(2,1)} %q_ref.1, bf16[256,384]{1,0:T(8,128)(2,1)} %f_ref.1, bf16[256,384]{1,0:T(8,128)(2,1)} %v_ref.1, bf16[256,384]{1,0:T(8,128)(2,1)} %g_ref.1, f32[1,384]{1,0:T(1,128)} %broadcast_in_dim.25.fmin_ref, f32[256,3]{1,0:T(8,128)} %bitcast.26, ...), custom_call_target="tpu_custom_call" | custom-call | flops 603979776 | bytes 3932160 | tf_op jit(solution)/shard_map/mixer/pallas_call | solution.py:272
  44.9 0.1 fusion.7
  45.0 1.6 convolution_convert_fusion
  46.6 55.1 %all_to_all.10 = bf16[8,32,3072]{2,1,0:T(8,128)(2,1)S(1)} all-to-all(bf16[8,32,3072]{2,1,0:T(8,128)(2,1)S(1)} %bitcast.23), channel_id=1, replica_groups=mesh['sp'=8,'tp'=4] {'sp'}, dimensions={0} | all-to-all | bytes 3145728 | tf_op jit(solution)/shard_map/all_to_all | solution.py:375
  101.7 4.6 %fusion.12 = f32[256,4,256]{2,0,1:T(8,128)S(1)} fusion(bf16[256,3072,1]{1,0,2:T(8,128)(2,1)S(1)} %bitcast.24, bf16[4,3072,256]{2,1,0:T(8,128)(2,1)} %all-gather.4.cloned.1.call-done), kind=kOutput, calls=%fused_computation.25 | convolution fusion | flops 1610612736 | bytes 8912896 | tf_op jit(solution)/shard_map/nd,tdf->tnf/dot_general | solution.py:379
  106.3 12.3 %all-gather.6.cloned.1.call-done = bf16[4,3072,256]{2,1,0:T(8,128)(2,1)} async-done(((bf16[1,3072,256]{2,1,0:T(8,128)(2,1)}), bf16[4,3072,256]{2,1,0:T(8,128)(2,1)}) %all-gather.6.cloned.1.call-update) | async-done | bytes 6291472 | tf_op jit(solution)/shard_map/all_gather | solution.py:349
  118.6 48.0 %all-gather.8.cloned.1.call-done = bf16[4,256,3072]{2,1,0:T(8,128)(2,1)} async-done(((bf16[1,256,3072]{2,1,0:T(8,128)(2,1)}), bf16[4,256,3072]{2,1,0:T(8,128)(2,1)}) %all-gather.8.cloned.1.call-update) | async-done | bytes 6291472 | tf_op jit(solution)/shard_map/all_gather | solution.py:350
  166.6 9.4 %fusion = bf16[256,3072]{1,0:T(8,128)(2,1)} fusion(bf16[4,256,3072]{2,1,0:T(8,128)(2,1)} %all-gather.8.cloned.1.call-done, bf16[256,3072,1]{1,0,2:T(8,128)(2,1)S(1)} %bitcast.25, bf16[4,3072,256]{2,1,0:T(8,128)(2,1)} %all-gather.6.cloned.1.call-done, f32[256,4,256]{2,0,1:T(8,128)S(1)} %fusion.12), kind=kOutput, calls=%fused_computation.1 | convolution fusion | flops 3223584768 | bytes 16777216 | tf_op jit(solution)/shard_map/dot_general | solution.py:384
  176.0 5.6 %all-to-all-start.1 = ((bf16[8,32,3072]{2,1,0:T(8,128)(2,1)}), bf16[8,32,3072]{2,1,0:T(8,128)(2,1)S(1)}, u32[]{:S(2)}, u32[]{:S(2)}) async-start(bf16[8,32,3072]{2,1,0:T(8,128)(2,1)} %bitcast.7), calls=%async_computation.1 | async-start | bytes 3145728 | tf_op jit(solution)/shard_map/all_to_all | solution.py:387
  181.6 0.0 copy-done.2
  181.6 0.1 select_reduce_fusion.1
  181.8 37.3 %all-to-all-done.1 = bf16[8,32,3072]{2,1,0:T(8,128)(2,1)S(1)} async-done(((bf16[8,32,3072]{2,1,0:T(8,128)(2,1)}), bf16[8,32,3072]{2,1,0:T(8,128)(2,1)S(1)}, u32[]{:S(2)}, u32[]{:S(2)}) %all-to-all-start.1) | async-done | bytes 1572896 | tf_op jit(solution)/shard_map/all_to_all | solution.py:387
  219.0 0.4 fusion.9
  219.4 1.2 fusion.2
  (14 shorter events, 0.1 us)
Async XLA Ops:
  6.5 95.1 %all-gather.4.cloned.1.call-start = ((), (), s32[]{:S(2)}) async-start(), calls=%async_computation.2 | async-start | bytes 7864320 | tf_op jit(solution)/shard_map/all_gather | solution.py:348
  7.3 1.5 copy-start.3
  7.3 111.3 %all-gather.6.cloned.1.call-start = ((), (), s32[]{:S(2)}) async-start(), calls=%async_computation.3 | async-start | bytes 7864320 | tf_op jit(solution)/shard_map/all_gather | solution.py:349
  8.0 2.0 copy-start.1
  8.0 2.8 %copy-start.4 = (f32[384]{0:T(512)S(1)}, f32[384]{0:T(512)}, u32[]{:S(2)}) copy-start(f32[384]{0:T(512)} %param.19) | copy-start | bytes 4612
  8.0 3.4 %copy-start.5 = (f32[384]{0:T(512)S(1)}, f32[384]{0:T(512)}, u32[]{:S(2)}) copy-start(f32[384]{0:T(512)} %param.21) | copy-start | bytes 4612
  8.0 158.5 %all-gather.8.cloned.1.call-start = ((), (), s32[]{:S(2)}) async-start(), calls=%async_computation.4 | async-start | bytes 7864320 | tf_op jit(solution)/shard_map/all_gather | solution.py:350
  175.9 5.7 %copy-start.2 = (f32[64,2]{0,1:T(2,128)S(1)}, f32[64,2]{0,1:T(2,128)}, u32[]{:S(2)}) copy-start(f32[64,2]{0,1:T(2,128)} %param.26) | copy-start | bytes 1540
  176.0 43.1 %all-to-all-start.1 = ((bf16[8,32,3072]{2,1,0:T(8,128)(2,1)}), bf16[8,32,3072]{2,1,0:T(8,128)(2,1)S(1)}, u32[]{:S(2)}, u32[]{:S(2)}) async-start(bf16[8,32,3072]{2,1,0:T(8,128)(2,1)} %bitcast.7), calls=%async_computation.1 | async-start | bytes 3145728 | tf_op jit(solution)/shard_map/all_to_all | solution.py:387
  181.6 37.8 %copy-start = (f32[64,3072]{1,0:T(8,128)S(1)}, f32[64,3072]{1,0:T(8,128)}, u32[]{:S(2)}) copy-start(f32[64,3072]{1,0:T(8,128)} %get-tuple-element.7) | copy-start | bytes 2359300
Sparse Core Ops, SparseCore 0:
  8.9 61.0 all-gather.3
  71.5 47.0 all-gather.5
  120.2 46.3 all-gather.7
where the time goes:
time: 227 us
  waiting for transfers between devices  99.6 us (44%)
  blocking collectives  55.1 us (24%)
  Pallas kernels  32.9 us (14%)
  matrix products  17.1 us (8%)
  between operations  13.2 us (6%)
  starting transfers between devices  5.73 us (3%)
  local copies, waits for them, and re-layouts  2.52 us (1%)
    all_to_all x1, blocking collectives, per_device(): lax.all_to_all(sendbuf.reshape(sp_size, capacity, -1), 'sp', split_axis=0...  55.1 us
    all_gather x1, waiting for transfers between devices, per_device(): down_all = lax.all_gather(expert_down_weight[0], 'tp')  48 us
    all_to_all x1, waiting for transfers between devices, per_device(): lax.all_to_all(expert_out.reshape(sp_size, capacity, -1), 'sp', split_axi...  37.3 us
    pallas_call x1, Pallas kernels, mixer(): pl.pallas_call(functools.partial(mixer_kernel, sp_size, tp_size), out_sha...  32.9 us
    all_gather x1, waiting for transfers between devices, per_device(): up_all = lax.all_gather(expert_up_weight[0], 'tp')  12.3 us
    dot_general x1, matrix products, per_device(): jnp.dot(inner_all, down_flat, preferred_element_type=jnp.float32)  9.38 us
    all_to_all x1, starting transfers between devices, per_device(): lax.all_to_all(expert_out.reshape(sp_size, capacity, -1), 'sp', split_axi...  5.65 us
    dot_general x1, matrix products, per_device(): jnp.einsum('nd,tdf->tnf', flat_rows, gate_all, preferred_element_type=jnp...  4.59 us
  transfers between devices with their start and end apart: 4, of which 3 were waited for; matrix products, arithmetic and copies ran while one was open for 4% of the time, Pallas kernels for 14%

commit v1 on v0

--- a/solution.py
+++ b/solution.py
@@ -318,11 +318,341 @@
     )
 
 
+def flip(index, step, size):
+    out = index
+    bit = 1
+    while bit < size:
+        out = out + bit * (lax.rem(lax.div(step, bit), 2)) * (1 - 2 * lax.rem(lax.div(index, bit), 2))
+        bit *= 2
+    return out
+
+
+def experts_kernel(
+    sp_size,
+    tp_size,
+    cap,
+    normed_ref,
+    residual_ref,
+    routes_ref,
+    score_ref,
+    gate_hbm,
+    up_hbm,
+    down_hbm,
+    out_ref,
+    table_ref,
+    weight_ref,
+    gu_ref,
+    down_ref,
+    send_ref,
+    rows_ref,
+    part_ref,
+    part_in,
+    own_ref,
+    xsum_ref,
+    xsum_in,
+    back_ref,
+    result_ref,
+    load_sem,
+    go_send,
+    go_recv,
+    sib_send,
+    sib_recv,
+    x_send,
+    x_recv,
+    relay_send,
+    relay_recv,
+    part_send,
+    part_recv,
+    xsum_send,
+    xsum_recv,
+    back_send,
+    back_recv,
+):
+    sp_me, tp_me = lax.axis_index("sp"), lax.axis_index("tp")
+    tokens, width = normed_ref.shape
+    hidden = down_ref.shape[0]
+    slots = sp_size * cap
+    sibling = tp_me + 1 - 2 * lax.rem(tp_me, 2)
+    across = lax.rem(tp_me + tp_size // 2, tp_size)
+
+    loads = [
+        pltpu.make_async_copy(gate_hbm.at[0], gu_ref.at[:, pl.ds(0, hidden)], load_sem.at[0]),
+        pltpu.make_async_copy(up_hbm.at[0], gu_ref.at[:, pl.ds(hidden, hidden)], load_sem.at[1]),
+        pltpu.make_async_copy(down_hbm.at[0], down_ref, load_sem.at[2]),
+    ]
+    for load in loads:
+        load.start()
+
+    barrier = pltpu.get_barrier_semaphore()
+    for k in range(1, sp_size):
+        pl.semaphore_signal(
+            barrier, inc=1, device_id=(flip(sp_me, k, sp_size), tp_me), device_id_type=MESH
+        )
+    for peer in (sibling, across):
+        pl.semaphore_signal(barrier, inc=1, device_id=(sp_me, peer), device_id_type=MESH)
+
+    own_routes = routes_ref[pl.ds(pl.multiple_of(tp_me * tokens, tokens), tokens), :]
+    lane = lax.broadcasted_iota(jnp.int32, (1, slots), 1)
+    step_of = lane // cap
+    expert = jnp.zeros((1, slots), jnp.int32)
+    bit = 1
+    while bit < sp_size:
+        mine = lax.rem(lax.div(sp_me, bit), 2)
+        theirs = (step_of // bit) % 2
+        expert = expert + bit * (theirs + mine - 2 * theirs * mine)
+        bit *= 2
+    first = own_routes[:, 0:1] == expert
+    second = own_routes[:, 1:2] == expert
+    named = jnp.where(first | second, 1.0, 0.0)
+    earlier = jnp.where(
+        lax.broadcasted_iota(jnp.int32, (tokens, tokens), 0)
+        > lax.broadcasted_iota(jnp.int32, (tokens, tokens), 1),
+        1.0,
+        0.0,
+    )
+    rank = jnp.dot(
+        earlier.astype(jnp.bfloat16),
+        named.astype(jnp.bfloat16),
+        preferred_element_type=jnp.float32,
+    )
+    hit = jnp.where(rank == (lane % cap).astype(jnp.float32), named, 0.0)
+    table_ref[...] = hit.astype(jnp.bfloat16)
+    score = score_ref[...]
+    share = score / jnp.sum(score, axis=1, keepdims=True)
+    weight = hit * jnp.where(first, share[:, 0:1], share[:, 1:2])
+    high = weight.astype(jnp.bfloat16)
+    weight_ref[:tokens, :] = high
+    weight_ref[tokens:, :] = (weight - high.astype(jnp.float32)).astype(jnp.bfloat16)
+
+    pl.semaphore_wait(barrier, sp_size + 1)
+
+    def go_copy(k):
+        return pltpu.make_async_remote_copy(
+            src_ref=send_ref.at[k],
+            dst_ref=rows_ref.at[k, 0],
+            send_sem=go_send.at[k],
+            recv_sem=go_recv.at[k],
+            device_id=(flip(sp_me, k, sp_size), tp_me),
+            device_id_type=MESH,
+        )
+
+    def tp_copy(src, dst, send_sem, recv_sem, peer):
+        return pltpu.make_async_remote_copy(
+            src_ref=src,
+            dst_ref=dst,
+            send_sem=send_sem,
+            recv_sem=recv_sem,
+            device_id=(sp_me, peer),
+            device_id_type=MESH,
+        )
+
+    def sib_copy(k):
+        return tp_copy(
+            rows_ref.at[k, 0], rows_ref.at[k, 1], sib_send.at[k], sib_recv.at[k], sibling
+        )
+
+    def x_copy(k):
+        return tp_copy(rows_ref.at[k, 0], rows_ref.at[k, 2], x_send.at[k], x_recv.at[k], across)
+
+    def relay_copy(k):
+        return tp_copy(
+            rows_ref.at[k, 2], rows_ref.at[k, 3], relay_send.at[k], relay_recv.at[k], sibling
+        )
+
+    def part_copy(k):
+        return tp_copy(
+            part_ref.at[k], part_in.at[k], part_send.at[k], part_recv.at[k], sibling
+        )
+
+    def xsum_copy(k):
+        return tp_copy(xsum_ref.at[k], xsum_in.at[k], xsum_send.at[k], xsum_recv.at[k], across)
+
+    def back_copy(k):
+        return pltpu.make_async_remote_copy(
+            src_ref=back_ref.at[k],
+            dst_ref=result_ref.at[k],
+            send_sem=back_send.at[k],
+            recv_sem=back_recv.at[k],
+            device_id=(flip(sp_me, k, sp_size), tp_me),
+            device_id_type=MESH,
+        )
+
+    group = max(1, min(sp_size, 128 // cap))
+    for first_k in range(0, sp_size, group):
+        picked = tn_dot(
+            table_ref[:, first_k * cap : (first_k + group) * cap], normed_ref[...]
+        ).astype(jnp.bfloat16)
+        for k in range(first_k, first_k + group):
+            block = picked[(k - first_k) * cap : (k - first_k + 1) * cap, :]
+            if k:
+                send_ref[k] = block
+                go_copy(k).start()
+            else:
+                rows_ref[0, 0] = block
+
+    def compute(k):
+        x = rows_ref[k].reshape(4 * cap, width)
+        both = jnp.dot(x, gu_ref[...], preferred_element_type=jnp.float32)
+        inner = (silu(both[:, :hidden]) * both[:, hidden:]).astype(jnp.bfloat16)
+        tile = width // 3 if width % 384 == 0 else width
+        for c in range(width // tile):
+            cols = slice(c * tile, (c + 1) * tile)
+            part = jnp.dot(inner, down_ref[:, cols], preferred_element_type=jnp.float32)
+            part_ref[k, 0, :, cols] = part[cap : 2 * cap].astype(jnp.bfloat16)
+            part_ref[k, 1, :, cols] = part[3 * cap :].astype(jnp.bfloat16)
+            own_ref[k, 0, :, cols] = part[:cap]
+            own_ref[k, 1, :, cols] = part[2 * cap : 3 * cap]
+
+    def body(i, carry):
+        @pl.when(i < sp_size)
+        def _():
+            @pl.when(i > 0)
+            def _():
+                go_copy(i).wait_recv()
+
+            x_copy(i).start()
+            sib_copy(i).start()
+
+        @pl.when((i >= 1) & (i < sp_size + 1))
+        def _():
+            k = i - 1
+            x_copy(k).wait_recv()
+            relay_copy(k).start()
+
+        @pl.when((i >= 3) & (i < sp_size + 3))
+        def _():
+            k = i - 3
+            part_copy(k).wait_recv()
+            xsum_ref[k] = (own_ref[k, 1] + part_in[k, 1].astype(jnp.float32)).astype(jnp.bfloat16)
+            xsum_copy(k).start()
+
+        @pl.when((i >= 2) & (i < sp_size + 2))
+        def _():
+            k = i - 2
+
+            @pl.when(k == 0)
+            def _():
+                for load in loads:
+                    load.wait()
+
+            sib_copy(k).wait_recv()
+            relay_copy(k).wait_recv()
+            compute(k)
+            part_copy(k).start()
+
+        @pl.when(i >= 4)
+        def _():
+            k = i - 4
+            xsum_copy(k).wait_recv()
+            final = (
+                own_ref[k, 0]
+                + part_in[k, 0].astype(jnp.float32)
+                + xsum_in[k].astype(jnp.float32)
+            ).astype(jnp.bfloat16)
+
+            @pl.when(k > 0)
+            def _():
+                back_ref[k] = final
+                back_copy(k).start()
+
+            @pl.when(k == 0)
+            def _():
+                result_ref[0] = final
+
+        return carry
+
+    lax.fori_loop(0, sp_size + 4, body, 0)
+
+    half = sp_size // 2
+    tile = width // 3 if width % 384 == 0 else width
+    for part in range(2):
+        for k in range(part * half, (part + 1) * half):
+            if k:
+                back_copy(k).wait_recv()
+        for c in range(width // tile):
+            cols = slice(c * tile, (c + 1) * tile)
+            rows = result_ref[part * half : (part + 1) * half, :, cols].reshape(half * cap, tile)
+            sums = jnp.dot(
+                weight_ref[:, part * half * cap : (part + 1) * half * cap],
+                rows,
+                preferred_element_type=jnp.float32,
+            )
+            total = sums[:tokens] + sums[tokens:] + residual_ref[:, cols]
+            if part:
+                out_ref[:, cols] = (total + own_ref[0, :, :, cols].reshape(2 * cap, tile)).astype(
+                    jnp.bfloat16
+                )
+            else:
+                own_ref[0, :, :, cols] = (sums[:tokens] + sums[tokens:]).reshape(2, cap, tile)
+
+    for k in range(sp_size):
+        if k:
+            go_copy(k).wait_send()
+            back_copy(k).wait_send()
+        sib_copy(k).wait_send()
+        x_copy(k).wait_send()
+        relay_copy(k).wait_send()
+        part_copy(k).wait_send()
+        xsum_copy(k).wait_send()
+
+
+def experts(normed, residual, routes, router_weight, gate, up, down):
+    sp_size, tp_size = lax.axis_size("sp"), lax.axis_size("tp")
+    tokens, width = normed.shape
+    cap = routes.shape[0] // sp_size
+    hidden = gate.shape[2]
+    slots = sp_size * cap
+    vmem = pl.BlockSpec(memory_space=pltpu.VMEM)
+    hbm = pl.BlockSpec(memory_space=pl.ANY)
+    dma = pltpu.SemaphoreType.DMA
+    low = jnp.bfloat16
+    return pl.pallas_call(
+        functools.partial(experts_kernel, sp_size, tp_size, cap),
+        out_shape=jax.ShapeDtypeStruct((tokens, width), low),
+        in_specs=[vmem] * 4 + [hbm] * 3,
+        out_specs=vmem,
+        scratch_shapes=[
+            pltpu.VMEM((tokens, slots), low),
+            pltpu.VMEM((2 * tokens, slots), low),
+            pltpu.VMEM((width, 2 * hidden), low),
+            pltpu.VMEM((hidden, width), low),
+            pltpu.VMEM((sp_size, cap, width), low),
+            pltpu.VMEM((sp_size, 4, cap, width), low),
+            pltpu.VMEM((sp_size, 2, cap, width), low),
+            pltpu.VMEM((sp_size, 2, cap, width), low),
+            pltpu.VMEM((sp_size, 2, cap, width), jnp.float32),
+            pltpu.VMEM((sp_size, cap, width), low),
+            pltpu.VMEM((sp_size, cap, width), low),
+            pltpu.VMEM((sp_size, cap, width), low),
+            pltpu.VMEM((sp_size, cap, width), low),
+            dma((3,)),
+        ]
+        + [dma((sp_size,))] * 14,
+        compiler_params=pltpu.CompilerParams(collective_id=1, has_side_effects=True),
+        cost_estimate=pl.CostEstimate(
+            flops=6 * 4 * slots * width * hidden,
+            bytes_accessed=6 * width * hidden,
+            transcendentals=4 * slots * hidden,
+        ),
+        name="experts",
+    )(normed, residual, routes, router_weight, gate, up, down)
+
+
 def dispatch_table(slot_ids, window_rows, quarter_rows):
     groups = slot_ids.shape[0]
     slot_grid = lax.broadcasted_iota(jnp.int32, (groups, window_rows, slot_ids.shape[1]), 1)
     hits = (slot_grid == slot_ids[:, None, :]).astype(jnp.bfloat16)
     return jnp.sum(hits.reshape(groups, window_rows, quarter_rows, TOPK), axis=3)
+
+
+def small_enough(sp_size, tp_size, capacity, tokens):
+    return (
+        tp_size == 4
+        and sp_size <= 16
+        and sp_size & (sp_size - 1) == 0
+        and capacity % 16 == 0
+        and tokens == 2 * capacity
+    )
 
 
 def per_device(
@@ -345,9 +675,6 @@
     window_rows = query.shape[0]
     tp_size = lax.axis_size("tp")
     sp_size = lax.axis_size("sp")
-    gate_all = lax.all_gather(expert_gate_weight[0], "tp")
-    up_all = lax.all_gather(expert_up_weight[0], "tp")
-    down_all = lax.all_gather(expert_down_weight[0], "tp")
     residual, normed = mixer(
         query,
         forget_preact,
@@ -362,6 +689,19 @@
     )
     quarter_rows = stream.shape[0]
     capacity = window_rows // sp_size
+    if small_enough(sp_size, tp_size, capacity, quarter_rows):
+        return experts(
+            normed,
+            residual,
+            routes,
+            router_weight,
+            expert_gate_weight,
+            expert_up_weight,
+            expert_down_weight,
+        )
+    gate_all = lax.all_gather(expert_gate_weight[0], "tp")
+    up_all = lax.all_gather(expert_up_weight[0], "tp")
+    down_all = lax.all_gather(expert_down_weight[0], "tp")
     pick_ids = routes.reshape(tp_size, quarter_rows * TOPK)
     onehot = (pick_ids[:, :, None] == jnp.arange(sp_size, dtype=jnp.int32)[None, None, :]).astype(
         jnp.int32

time: 227 us -> 142 us (0.63)
  the two profiles are of different devices: /device:TPU:0 before, /device:TPU:8 now
where the time goes in v1:
time: 142 us
  Pallas kernels  134 us (94%)
  local copies, waits for them, and re-layouts  8.56 us (6%)
    pallas_call x1, Pallas kernels, experts(): pl.pallas_call(functools.partial(experts_kernel, sp_size, tp_size, cap),...  108 us
    pallas_call x1, Pallas kernels, mixer(): pl.pallas_call(functools.partial(mixer_kernel, sp_size, tp_size), out_sha...  25.4 us
    unnamed x4, local copies, waits for them, and re-layouts  6.09 us

profile of v1, /device:TPU:8, one launch (start us, length us, event | category | flops | bytes accessed | tf_op | source)
XLA Modules:
  0.0 142.1 jit_solution(2073294706503825987)
XLA Ops:
  0.0 1.2 broadcast_in_dim.9.fmin_ref
  1.2 1.2 broadcast_in_dim.10.gain_ref
  2.5 1.4 copy.18.score_ref
  3.8 1.5 %copy.16 = f32[3,256]{0,1:T(8,128)} copy(f32[3,256]{1,0:T(4,128)} %param.20) | data formatting | bytes 6144 | tf_op args[5]
  5.3 1.5 %copy.17.routes_ref = s32[256,2]{1,0:T(8,128)} copy(s32[256,2]{0,1:T(2,128)} %param.25) | data formatting | bytes 4096 | tf_op args[10]
  6.8 25.4 %mixer.1 = (f32[64,3072]{1,0:T(8,128)}, bf16[64,3072]{1,0:T(8,128)(2,1)}) custom-call(bf16[256,384]{1,0:T(8,128)(2,1)} %q_ref.1, bf16[256,384]{1,0:T(8,128)(2,1)} %f_ref.1, bf16[256,384]{1,0:T(8,128)(2,1)} %v_ref.1, bf16[256,384]{1,0:T(8,128)(2,1)} %g_ref.1, f32[1,384]{1,0:T(1,128)} %broadcast_in_dim.9.fmin_ref, f32[256,3]{1,0:T(8,128)} %bitcast.2, ...), custom_call_target="tpu_custom_call" | custom-call | flops 603979776 | bytes 3932160 | tf_op jit(solution)/shard_map/mixer/pallas_call | solution.py:272
  32.2 108.1 %experts.1 = bf16[64,3072]{1,0:T(8,128)(2,1)} custom-call(bf16[64,3072]{1,0:T(8,128)(2,1)} %get-tuple-element.7.normed_ref, f32[64,3072]{1,0:T(8,128)} %get-tuple-element.8.residual_ref, s32[256,2]{1,0:T(8,128)} %copy.17.routes_ref, f32[64,2]{1,0:T(8,128)} %copy.18.score_ref, bf16[1,3072,256]{2,1,0:T(8,128)(2,1)} %gate_hbm.1, bf16[1,3072,256]{2,1,0:T(8,128)(2,1)} %up_hbm.1, ...), custom_call_target="tpu_custom_call" | custom-call | flops 4831838208 | bytes 4718592 | tf_op jit(solution)/shard_map/experts/pallas_call | solution.py:609
  140.4 1.8 %copy.20 = bf16[64,3072]{1,0:T(8,128)(2,1)} copy(bf16[64,3072]{1,0:T(8,128)(2,1)} %experts.1) | data formatting | bytes 786432
